TPU v7x, 32 devices: a whole 2x2x4 slice. The times are simulated.
32 devices in a mesh: grp: 2 (over x), ep: 16 (over z, y, core).
Axes of the slice: x: 2, y: 2, z: 4, core: 2. Of those that a mesh axis runs over, the one named last changes fastest.
Arguments:
- tokens: bfloat16 [4096, 2048], P(('grp', 'ep')), parts along dimension 0, may hold values from -6 to 6
- norm_gain: float32 [2048], replicated, may hold values from 0.1 to 1.9
- expert_ids: int32 [4096, 2], P(('grp', 'ep')), parts along dimension 0, may hold values from 0 to 3, all different within a row; in each aligned block of 128 rows (0 to 127, 128 to 255, ...) at most 128 rows name the same one
- route_weight: float32 [4096, 2], P(('grp', 'ep')), parts along dimension 0, may hold values from 0.1 to 1
- gate_weight: bfloat16 [16, 2048, 512], P('ep'), may hold values from -0.375 to 0.375
- up_weight: bfloat16 [16, 2048, 512], P('ep'), may hold values from -0.375 to 0.375
- down_weight: bfloat16 [16, 512, 2048], P('ep'), may hold values from -0.03125 to 0.03125
Outputs:
- combined: bfloat16 [4096, 2048], P(('grp', 'ep')), parts along dimension 0
There are 2 independent parts, one for each index of `grp`. A program takes and returns all parts, laid end to end along the dimension named above; an argument that names none is the same for every part. Nothing has to cross between parts.
Inputs may be any that keep to these rules, and one draw needn't show every extreme that they name: `expert_ids`: each token names 2 different experts; among the tokens of one device no expert is named more than 128 times, and in every draw some expert is named exactly 128 times by the tokens of some device.
All inputs are finite; a program needn't handle non-finite values.
Results may differ from a plain program's by a relative error of at most 0.0078.
Values may be sent and summed in bfloat16 or wider, within the bound.
A program may use at most 128 MiB of HBM per device.

v0:
```python
import functools

import jax
import jax.numpy as jnp
from jax import lax
from jax.experimental import pallas as pl
from jax.experimental.pallas import tpu as pltpu
from jax.sharding import PartitionSpec as P

SPLIT = 4


EPSILON = 1e-05
clamp_limit = 7.0
sigmoid_slope = 1.702


def swapped(array, axis, bit):
    return lax.ppermute(array, axis, [(i, i ^ 1 << bit) for i in range(lax.axis_size(axis))])


def layer_norm(tokens, norm_gain):
    values = tokens.astype(jnp.float32)
    center = values - jnp.mean(values, axis=-1, keepdims=True)
    spread = jnp.mean(center * center, axis=-1, keepdims=True)
    return (center * lax.rsqrt(spread + EPSILON) * norm_gain).astype(jnp.bfloat16)


def expert_rows(block_rows, gate_weight, up_weight, down_weight):
    gate_pre = jnp.einsum(
        "scd,df->scf", block_rows, gate_weight[0], preferred_element_type=jnp.float32
    )
    up_pre = jnp.einsum("scd,df->scf", block_rows, up_weight[0], preferred_element_type=jnp.float32)
    gate_cut = jnp.minimum(gate_pre, clamp_limit)
    up_cut = jnp.clip(up_pre, -clamp_limit, clamp_limit)
    active = ((up_cut + 1.0) * (gate_cut * jax.nn.sigmoid(gate_cut * sigmoid_slope))).astype(
        jnp.bfloat16
    )
    return jnp.einsum("scf,fd->scd", active, down_weight[0], preferred_element_type=jnp.float32)


def slot_body(tokens, norm_gain, expert_ids, route_weight, gate_weight, up_weight, down_weight):
    normed = layer_norm(tokens, norm_gain)
    devices = lax.axis_size("ep")
    experts = devices // SPLIT
    tok_rows = tokens.shape[0]
    top_count = expert_ids.shape[1]
    width = tokens.shape[1]
    capacity = min(tok_rows, 2 * tok_rows * top_count // experts)
    quarter = capacity // SPLIT
    levels = SPLIT.bit_length() - 1
    position = lax.axis_index("ep")
    flat_ids = expert_ids.reshape(-1)
    onehot = (flat_ids[:, None] == jnp.arange(experts, dtype=jnp.int32)[None, :]).astype(jnp.int32)
    earlier = jnp.cumsum(onehot, axis=0) - onehot
    slot_index = jnp.sum(earlier * onehot, axis=1)
    target = flat_ids * capacity + slot_index
    owners = jnp.arange(flat_ids.shape[0], dtype=jnp.int32) // top_count
    slot_token = jnp.full((experts * capacity,), tok_rows, jnp.int32).at[target].set(owners)
    padded = jnp.concatenate([normed, jnp.zeros((1, width), jnp.bfloat16)], axis=0)
    outgoing = jnp.take(padded, slot_token, axis=0).reshape(experts, capacity, width)
    pieces = outgoing.reshape(devices, quarter, width)
    gathered = lax.all_to_all(pieces, "ep", split_axis=0, concat_axis=0, tiled=True)
    for bit_level in range(levels):
        partner = swapped(gathered, "ep", bit_level)
        upper_bit = position >> bit_level & 1
        first_half = jnp.where(upper_bit == 1, partner, gathered)
        second_half = jnp.where(upper_bit == 1, gathered, partner)
        gathered = jnp.concatenate([first_half, second_half], axis=1)
    partial_value = expert_rows(gathered, gate_weight, up_weight, down_weight)
    length = capacity
    for bit_level in reversed(range(levels)):
        length = length // 2
        upper_bit = position >> bit_level & 1
        kept_rows = lax.dynamic_slice_in_dim(partial_value, upper_bit * length, length, 1)
        sent_rows = lax.dynamic_slice_in_dim(partial_value, (1 - upper_bit) * length, length, 1)
        partial_value = kept_rows + swapped(sent_rows, "ep", bit_level)
    finished = partial_value.astype(jnp.bfloat16)
    returned = lax.all_to_all(finished, "ep", split_axis=0, concat_axis=0, tiled=True)
    results = returned.reshape(experts * capacity, width)
    picked = jnp.take(results, target, axis=0).reshape(tok_rows, top_count, width)
    combined = jnp.sum(route_weight[:, :, None] * picked.astype(jnp.float32), axis=1)
    return combined.astype(jnp.bfloat16)


MESH = pl.DeviceIdType.MESH
HALVES = 2
LANES = 128


def near_plane(z, k, planes):
    below, above = z, planes - 1 - z
    short = jnp.minimum(below, above)
    side = jnp.where(above >= below, 1, -1)
    paired = jnp.where(k % 2 == 1, side * ((k + 1) // 2), -side * (k // 2))
    return z + jnp.where(k <= 2 * short, paired, side * (k - short))


def lane_to_column(row, rows):
    eye = lax.broadcasted_iota(jnp.int32, (rows, rows), 0) == lax.broadcasted_iota(
        jnp.int32, (rows, rows), 1
    )
    return jnp.sum(jnp.where(eye, row, 0.0), axis=1, keepdims=True)


def dense_kernel(
    devices,
    tokens_ref, gain_ref, ids_ref, route_ref, gate_hbm, up_hbm, down_hbm,
    out_ref,
    tok, part, cbuf, ybuf, zbuf, acc, gate, up, down,
    wsem, gsend, grecv, rsend_c, rrecv_c, rsend_y, rrecv_y, rsend_z, rrecv_z,
):
    planes = devices // SPLIT
    rows, width = tokens_ref.shape
    half = rows // HALVES
    me = lax.axis_index("ep")
    z, y, c = me // 4, (me // 2) % 2, me % 2

    def index(zp, yp, cp):
        return zp * 4 + yp * 2 + cp

    ypeer, cpeer = index(z, 1 - y, c), index(z, y, 1 - c)

    def span(h):
        return pl.ds(h * half, half)

    def remote(source, target, send_sem, recv_sem, device):
        return pltpu.make_async_remote_copy(
            src_ref=source, dst_ref=target, send_sem=send_sem, recv_sem=recv_sem,
            device_id={"ep": device}, device_id_type=MESH,
        )

    def move(kind, i, h, device):
        return remote(
            tok.at[i, span(h)], tok.at[i, span(h)], gsend.at[kind, i, h], grecv.at[i, h], device
        )

    weight_loads = [
        pltpu.make_async_copy(gate_hbm.at[0], gate, wsem.at[0]),
        pltpu.make_async_copy(up_hbm.at[0], up, wsem.at[1]),
        pltpu.make_async_copy(down_hbm.at[0], down, wsem.at[2]),
    ]
    for load in weight_loads:
        load.start()

    has_up, has_down = z < planes - 1, z > 0
    barrier = pltpu.get_barrier_semaphore()

    def greet(device):
        pl.semaphore_signal(
            barrier, inc=1, device_id={"ep": device}, device_id_type=MESH
        )

    greet(ypeer)
    greet(cpeer)
    pl.when(has_up)(lambda: greet(me + 4))
    pl.when(has_down)(lambda: greet(me - 4))

    lanes = lax.broadcasted_iota(jnp.int32, (1, LANES), 1)
    routes = jnp.zeros((rows, LANES), jnp.float32)
    for e in range(planes):
        row = jnp.sum(jnp.where(ids_ref[...] == e, route_ref[...], 0.0), axis=0, keepdims=True)
        column = lane_to_column(row, rows)
        high = column.astype(jnp.bfloat16).astype(jnp.float32)
        routes = jnp.where(lanes == e, high, routes)
        routes = jnp.where(lanes == planes + e, column - high, routes)
    tok[me, :, width:] = routes.astype(jnp.bfloat16)
    for h in range(HALVES):
        values = tokens_ref[span(h), :].astype(jnp.float32)
        center = values - jnp.mean(values, axis=-1, keepdims=True)
        spread = jnp.mean(center * center, axis=-1, keepdims=True)
        tok[me, span(h), :width] = (center * lax.rsqrt(spread + EPSILON) * gain_ref[...]).astype(
            jnp.bfloat16
        )
        if h == 0:
            pl.semaphore_wait(
                barrier, 2 + has_up.astype(jnp.int32) + has_down.astype(jnp.int32)
            )
        move(2, me, h, ypeer).start()
        pl.when(has_up)(lambda: move(0, me, h, me + 4).start())
        pl.when(has_down)(lambda: move(1, me, h, me - 4).start())
        move(3, me, h, cpeer).start()
    for load in weight_loads:
        load.wait()

    def onward(zp):
        return jnp.where(zp < z, z + 1, z - 1)

    def exists(plane):
        return jnp.logical_and(plane >= 0, plane < planes)

    def compute(zp, yp):
        first = index(zp, yp, 0)
        x = tok[pl.ds(first, 2), :, :width].reshape(2 * rows, width)
        routes = tok[pl.ds(first, 2), :, width:].reshape(2 * rows, LANES).astype(jnp.float32)
        gate_cut = jnp.minimum(
            jnp.dot(x, gate[...], preferred_element_type=jnp.float32), clamp_limit
        )
        up_cut = jnp.clip(
            jnp.dot(x, up[...], preferred_element_type=jnp.float32), -clamp_limit, clamp_limit
        )
        active = ((up_cut + 1.0) * (gate_cut * jax.nn.sigmoid(gate_cut * sigmoid_slope))).astype(
            jnp.bfloat16
        )
        mine = jnp.logical_or(lanes == z, lanes == planes + z)
        scale = jnp.sum(jnp.where(mine, routes, 0.0), axis=1, keepdims=True)
        tile = min(512, width)
        for start in range(0, width, tile):
            value = jnp.dot(
                active, down[:, start : start + tile], preferred_element_type=jnp.float32
            )
            part[pl.ds(first, 2), :, start : start + tile] = (
                (value * scale).astype(jnp.bfloat16).reshape(2, rows, tile)
            )

    def to_core(zp, yp):
        pair = zp * 2 + yp
        return remote(
            part.at[index(zp, yp, 1 - c)], cbuf.at[pair],
            rsend_c.at[pair], rrecv_c.at[pair], cpeer,
        )

    def beside(plane):
        return jnp.abs(plane - z) == 1

    def pass_up():
        return move(4, index(z, 1 - y, c), 1, me + 4)

    def pass_down():
        return move(5, index(z, 1 - y, c), 1, me - 4)

    def take(i, h):
        move(3, i, h, cpeer).wait_recv()
        move(3, i, h, cpeer).start()

    def group(zp, yp):
        for h in range(HALVES):
            move(3, index(zp, yp, 1 - c), h, cpeer).wait_recv()
        compute(zp, yp)
        to_core(zp, yp).start()

    def to_y(zp, h):
        return remote(
            part.at[index(zp, 1 - y, c), span(h)], ybuf.at[zp, span(h)],
            rsend_y.at[zp, h], rrecv_y.at[zp, h], ypeer,
        )

    def spread_half(zp, h):
        i = index(zp, 1 - y, c)
        part[i, span(h), :] = (
            part[i, span(h), :].astype(jnp.float32)
            + cbuf[zp * 2 + 1 - y, span(h), :].astype(jnp.float32)
        ).astype(jnp.bfloat16)
        to_y(zp, h).start()

    def gather_step(k, _):
        zk = near_plane(z, jnp.minimum(k, planes - 1), planes)
        zb = near_plane(z, jnp.maximum(k - 1, 0), planes)

        @pl.when(k == planes)
        def _():
            to_core(z, 1 - y).wait_recv()
            spread_half(z, 0)

        @pl.when(jnp.logical_and(k > 0, k < planes))
        def _():
            i = index(zk, y, c)
            nz = onward(zk)
            for h in range(HALVES):
                move(2, i, h, ypeer).wait_recv()
                pl.when(exists(nz))(lambda: move(0, i, h, index(nz, y, c)).start())
                if h == 0:
                    move(2, i, h, ypeer).start()
                else:
                    pl.when(jnp.logical_not(beside(zk)))(lambda: move(2, i, h, ypeer).start())
                move(3, i, h, cpeer).start()

        @pl.when(k == planes - 1)
        def _():
            inner = jnp.logical_and(has_up, has_down)
            pl.when(inner)(lambda: pass_up().start())
            pl.when(inner)(lambda: pass_down().start())

        @pl.when(k > 0)
        def _():
            i = index(zb, 1 - y, c)
            take(i, 0)
            pl.when(jnp.logical_not(beside(zb)))(lambda: take(i, 1))

        @pl.when(k == 1)
        def _():
            pl.when(jnp.logical_not(has_down))(lambda: pass_up().start())
            pl.when(jnp.logical_not(has_up))(lambda: pass_down().start())

        def group_step(j, _):
            zp = jnp.where(j == 0, zk, zb)
            yp = jnp.where(j == 0, y, 1 - y)
            ready = jnp.where(beside(zb), 0, k)
            pl.when(jnp.where(j == 0, planes - k, ready) > 0)(lambda: group(zp, yp))
            return 0

        lax.fori_loop(0, 2, group_step, 0)
        return 0

    lax.fori_loop(0, planes + 1, gather_step, 0)

    def from_y(zp, h):
        return remote(
            part.at[index(zp, y, c), span(h)], ybuf.at[zp, span(h)],
            rsend_y.at[zp, h], rrecv_y.at[zp, h], ypeer,
        )

    def spread_step(t, _):
        zp = near_plane(z, planes - 1 - t, planes)
        i = index(zp, 1 - y, c)

        @pl.when(beside(zp))
        def _():
            take(i, 1)
            group(zp, 1 - y)

        @pl.when(zp != z)
        def _():
            to_core(zp, 1 - y).wait_recv()
            spread_half(zp, 0)

        spread_half(zp, 1)
        return 0

    lax.fori_loop(0, planes, spread_step, 0)

    def hop(zp, h):
        nz = jnp.where(zp > z, z + 1, z - 1)
        slot = jnp.where(jnp.logical_and(nz == zp, zp < z), planes, zp)
        return remote(
            part.at[index(zp, y, c), span(h)], zbuf.at[slot, span(h)],
            rsend_z.at[zp, h], rrecv_z.at[slot, h], index(nz, y, c),
        )

    def landed(slot, h):
        return remote(
            part.at[me, span(h)], zbuf.at[slot, span(h)],
            rsend_z.at[z, h], rrecv_z.at[slot, h], ypeer,
        )

    def add_landed(slot, h):
        landed(slot, h).wait_recv()
        acc[...] += zbuf[slot, span(h), :].astype(jnp.float32)

    def total(zp, h):
        from_y(zp, h).wait_recv()
        acc[...] = (
            part[index(zp, y, c), span(h), :].astype(jnp.float32)
            + cbuf[zp * 2 + y, span(h), :].astype(jnp.float32)
            + ybuf[zp, span(h), :].astype(jnp.float32)
        )

    def chain_step(t, _):
        zp = near_plane(z, planes - 1 - t, planes)
        to_core(zp, y).wait_recv()
        for h in range(HALVES):
            total(zp, h)
            pl.when(jnp.where(zp > z, has_down, has_up))(lambda: add_landed(zp, h))
            part[index(zp, y, c), span(h), :] = acc[...].astype(jnp.bfloat16)
            hop(zp, h).start()
        return 0

    lax.fori_loop(0, planes - 1, chain_step, 0)
    to_core(z, y).wait_recv()
    for h in range(HALVES):
        total(z, h)
        pl.when(has_down)(lambda: add_landed(z, h))
        pl.when(has_up)(lambda: add_landed(planes, h))
        out_ref[span(h), :] = acc[...].astype(jnp.bfloat16)

    for h in range(HALVES):
        move(2, me, h, ypeer).wait_send()
        pl.when(has_up)(lambda: move(0, me, h, me + 4).wait_send())
        pl.when(has_down)(lambda: move(1, me, h, me - 4).wait_send())
        move(3, me, h, cpeer).wait_send()

    pl.when(has_up)(lambda: pass_up().wait_send())
    pl.when(has_down)(lambda: pass_down().wait_send())

    def drain_step(k, _):
        zp = near_plane(z, k, planes)
        to_core(zp, y).wait_send()
        to_core(zp, 1 - y).wait_send()
        for h in range(HALVES):
            move(3, index(zp, 1 - y, c), h, cpeer).wait_send()
            to_y(zp, h).wait_send()

        @pl.when(k > 0)
        def _():
            i = index(zp, y, c)
            nz = onward(zp)
            for h in range(HALVES):
                pl.when(exists(nz))(lambda: move(0, i, h, index(nz, y, c)).wait_send())
                if h == 0:
                    move(2, i, h, ypeer).wait_send()
                else:
                    pl.when(jnp.logical_not(beside(zp)))(
                        lambda: move(2, i, h, ypeer).wait_send()
                    )
                move(3, i, h, cpeer).wait_send()
                hop(zp, h).wait_send()

        return 0

    lax.fori_loop(0, planes, drain_step, 0)


def dense_body(tokens, norm_gain, expert_ids, route_weight, gate_weight, up_weight, down_weight):
    devices = lax.axis_size("ep")
    planes = devices // SPLIT
    rows, width = tokens.shape
    hidden = gate_weight.shape[2]
    half = rows // HALVES
    vmem, dma = pltpu.VMEM, pltpu.SemaphoreType.DMA
    block = jnp.bfloat16
    return pl.pallas_call(
        functools.partial(dense_kernel, devices),
        out_shape=jax.ShapeDtypeStruct((rows, width), block),
        in_specs=[pl.BlockSpec(memory_space=vmem)] * 4 + [pl.BlockSpec(memory_space=pl.ANY)] * 3,
        out_specs=pl.BlockSpec(memory_space=vmem),
        scratch_shapes=[
            vmem((devices, rows, width + LANES), block),
            vmem((devices, rows, width), block),
            vmem((2 * planes, rows, width), block),
            vmem((planes, rows, width), block),
            vmem((planes + 1, rows, width), block),
            vmem((half, width), jnp.float32),
            vmem((width, hidden), block),
            vmem((width, hidden), block),
            vmem((hidden, width), block),
            dma((3,)),
            dma((6, devices, HALVES)),
            dma((devices, HALVES)),
            dma((2 * planes,)),
            dma((2 * planes,)),
            dma((planes, HALVES)),
            dma((planes, HALVES)),
            dma((planes, HALVES)),
            dma((planes + 1, HALVES)),
        ],
        compiler_params=pltpu.CompilerParams(
            collective_id=0, has_side_effects=True, vmem_limit_bytes=60 * 1024 * 1024
        ),
        name="dense_experts",
    )(
        tokens, norm_gain.reshape(1, width), expert_ids.T, route_weight.T,
        gate_weight, up_weight, down_weight,
    )


def body(tokens, norm_gain, expert_ids, route_weight, gate_weight, up_weight, down_weight):
    tok_rows, top_count = expert_ids.shape
    experts = lax.axis_size("ep") // SPLIT
    capacity = min(tok_rows, 2 * tok_rows * top_count // experts)
    chosen = dense_body if capacity == tok_rows else slot_body
    return chosen(
        tokens, norm_gain, expert_ids, route_weight, gate_weight, up_weight, down_weight
    )


def solution(mesh):
    placed = (
        P(("grp", "ep"), None),
        P(),
        P(("grp", "ep"), None),
        P(("grp", "ep"), None),
        P("ep", None, None),
        P("ep", None, None),
        P("ep", None, None),
    )
    return jax.shard_map(
        body, mesh=mesh, in_specs=placed, out_specs=P(("grp", "ep"), None), check_vma=False
    )
```

profile of v0, /device:TPU:0, one launch (start us, length us, event | category | flops | bytes accessed | tf_op | source)
XLA Modules:
  0.0 103.8 jit_solution(14411358850814133020)
XLA Ops:
  0.0 101.9 %dense_experts.1 = bf16[128,2048]{1,0:T(8,128)(2,1)} custom-call(bf16[128,2048]{1,0:T(8,128)(2,1)} %tokens_ref.1, f32[1,2048]{1,0:T(1,128)} %bitcast.3, s32[2,128]{1,0:T(2,128)} %bitcast.4, f32[2,128]{1,0:T(2,128)} %bitcast.5, bf16[1,2048,512]{2,1,0:T(8,128)(2,1)} %gate_hbm.1, bf16[1,2048,512]{2,1,0:T(8,128)(2,1)} %up_hbm.1, bf16[1,512,2048]{2,1,0:T(8,128)(2,1)} %down_hbm.1), custom_call_target="tpu_custom_call" | custom-call | tf_op jit(solution)/shard_map/dense_experts/pallas_call | solution.py:421
  101.9 1.9 %copy.9 = bf16[128,2048]{1,0:T(8,128)(2,1)} copy(bf16[128,2048]{1,0:T(8,128)(2,1)} %dense_experts.1) | data formatting | bytes 1048576
where the time goes:
time: 104 us
  Pallas kernels  102 us (98%)
  local copies, waits for them, and re-layouts  1.88 us (2%)
    pallas_call x1, Pallas kernels, dense_body(): pl.pallas_call(functools.partial(dense_kernel, devices), out_shape=jax.Sh...  102 us

commit v1 on v0

v1 whole, which is shorter than its diff:
```python
import functools

import jax
import jax.numpy as jnp
from jax import lax
from jax.experimental import pallas as pl
from jax.experimental.pallas import tpu as pltpu
from jax.sharding import PartitionSpec as P

SPLIT = 4


EPSILON = 1e-05
clamp_limit = 7.0
sigmoid_slope = 1.702


def swapped(array, axis, bit):
    return lax.ppermute(array, axis, [(i, i ^ 1 << bit) for i in range(lax.axis_size(axis))])


def layer_norm(tokens, norm_gain):
    values = tokens.astype(jnp.float32)
    center = values - jnp.mean(values, axis=-1, keepdims=True)
    spread = jnp.mean(center * center, axis=-1, keepdims=True)
    return (center * lax.rsqrt(spread + EPSILON) * norm_gain).astype(jnp.bfloat16)


def expert_rows(block_rows, gate_weight, up_weight, down_weight):
    gate_pre = jnp.einsum(
        "scd,df->scf", block_rows, gate_weight[0], preferred_element_type=jnp.float32
    )
    up_pre = jnp.einsum("scd,df->scf", block_rows, up_weight[0], preferred_element_type=jnp.float32)
    gate_cut = jnp.minimum(gate_pre, clamp_limit)
    up_cut = jnp.clip(up_pre, -clamp_limit, clamp_limit)
    active = ((up_cut + 1.0) * (gate_cut * jax.nn.sigmoid(gate_cut * sigmoid_slope))).astype(
        jnp.bfloat16
    )
    return jnp.einsum("scf,fd->scd", active, down_weight[0], preferred_element_type=jnp.float32)


def slot_body(tokens, norm_gain, expert_ids, route_weight, gate_weight, up_weight, down_weight):
    normed = layer_norm(tokens, norm_gain)
    devices = lax.axis_size("ep")
    experts = devices // SPLIT
    tok_rows = tokens.shape[0]
    top_count = expert_ids.shape[1]
    width = tokens.shape[1]
    capacity = min(tok_rows, 2 * tok_rows * top_count // experts)
    quarter = capacity // SPLIT
    levels = SPLIT.bit_length() - 1
    position = lax.axis_index("ep")
    flat_ids = expert_ids.reshape(-1)
    onehot = (flat_ids[:, None] == jnp.arange(experts, dtype=jnp.int32)[None, :]).astype(jnp.int32)
    earlier = jnp.cumsum(onehot, axis=0) - onehot
    slot_index = jnp.sum(earlier * onehot, axis=1)
    target = flat_ids * capacity + slot_index
    owners = jnp.arange(flat_ids.shape[0], dtype=jnp.int32) // top_count
    slot_token = jnp.full((experts * capacity,), tok_rows, jnp.int32).at[target].set(owners)
    padded = jnp.concatenate([normed, jnp.zeros((1, width), jnp.bfloat16)], axis=0)
    outgoing = jnp.take(padded, slot_token, axis=0).reshape(experts, capacity, width)
    pieces = outgoing.reshape(devices, quarter, width)
    gathered = lax.all_to_all(pieces, "ep", split_axis=0, concat_axis=0, tiled=True)
    for bit_level in range(levels):
        partner = swapped(gathered, "ep", bit_level)
        upper_bit = position >> bit_level & 1
        first_half = jnp.where(upper_bit == 1, partner, gathered)
        second_half = jnp.where(upper_bit == 1, gathered, partner)
        gathered = jnp.concatenate([first_half, second_half], axis=1)
    partial_value = expert_rows(gathered, gate_weight, up_weight, down_weight)
    length = capacity
    for bit_level in reversed(range(levels)):
        length = length // 2
        upper_bit = position >> bit_level & 1
        kept_rows = lax.dynamic_slice_in_dim(partial_value, upper_bit * length, length, 1)
        sent_rows = lax.dynamic_slice_in_dim(partial_value, (1 - upper_bit) * length, length, 1)
        partial_value = kept_rows + swapped(sent_rows, "ep", bit_level)
    finished = partial_value.astype(jnp.bfloat16)
    returned = lax.all_to_all(finished, "ep", split_axis=0, concat_axis=0, tiled=True)
    results = returned.reshape(experts * capacity, width)
    picked = jnp.take(results, target, axis=0).reshape(tok_rows, top_count, width)
    combined = jnp.sum(route_weight[:, :, None] * picked.astype(jnp.float32), axis=1)
    return combined.astype(jnp.bfloat16)


MESH = pl.DeviceIdType.MESH
PLANES = 4
PIECES = 4

RELAY, CROSS, COMPUTE, SETTLE = 0, 1, 2, 3
GROUP = 8
END_WORDS = (
    32897, 262209, 335609865, 2373642, 13631520, 11534409,
    6341706, 1312779, 557072, 69566664, 6612242, 7340112,
    3408008, 67731480, 170459161, 68517936, 7110872, 2657386,
    69828745, 300744936, 1837163, 5347714, 8126648, 74311474,
    6815864, 201130096, 68780272, 121438267, 75333784, 259063995,
    4032627, 166264920, 5767411, 1149211, 98109851, 5505168,
    5870058, 82413915, 7706002, 80314539, 82150115, 80052835,
    230791939, 228694979,
)
MID_WORDS = (
    6586377, 8388648, 279248897, 557584, 19411242, 14680201,
    6340810, 17563680, 7602592, 11534361, 1573592, 23606306,
    10485969, 300744921, 2654264, 22806912, 20709800, 245965522,
    101297978, 24641609, 5344442, 69042424, 3670680, 7700704,
    103388610, 3408472, 326697648, 21495931, 6131811, 263785691,
    102335011, 108893786, 239927539, 104436419, 111216171, 5868571,
    158438018, 53841307, 112041739, 115970819, 5608323, 113876811,
    266703427, 139147,
)
END_SENT = (12, 6, 0, 32, 32, 28)
END_TILES = (4, 1, 0, 8)
MID_SENT = (11, 11, 16, 32, 32, 28)
MID_TILES = (4, 2, 3, 8)


def lane_column(row, piece, rows):
    lanes = lax.broadcasted_iota(jnp.int32, (rows, row.shape[1]), 1)
    line = lax.broadcasted_iota(jnp.int32, (rows, row.shape[1]), 0)
    return jnp.sum(jnp.where(lanes == piece * rows + line, row, 0.0), axis=1, keepdims=True)


def dense_kernel(
    tokens_ref, gain_ref, ids_ref, route_ref, gate_hbm, up_hbm, down_hbm,
    out_ref,
    tok, part, cbuf, ybuf, zbuf, acc, routes, gate, up, down,
    wsem, arrived, routed, shared, crossed, climbed, sent, rsent,
):
    rows, width = tokens_ref.shape
    piece_rows = rows // PIECES
    me = lax.axis_index("ep")
    z, y, c = me // 4, (me // 2) % 2, me % 2
    flipped = (z >= PLANES // 2).astype(jnp.int32)
    level = jnp.where(z >= PLANES // 2, PLANES - 1 - z, z)
    is_end = level == 0
    upward = 1 - 2 * flipped
    ypeer, cpeer = z * 4 + (1 - y) * 2 + c, z * 4 + y * 2 + 1 - c
    above, below = me + 4 * upward, me - 4 * upward

    def plane_of(h):
        return jnp.where(z >= PLANES // 2, PLANES - 1 - h, h)

    def column_of(o):
        return jnp.where(o == 0, y, 1 - y)

    def remote(source, target, send_sem, recv_sem, device):
        return pltpu.make_async_remote_copy(
            src_ref=source, dst_ref=target, send_sem=send_sem, recv_sem=recv_sem,
            device_id={"ep": device}, device_id_type=MESH,
        )

    def move(kind, slot, device):
        return remote(tok.at[slot], tok.at[slot], sent.at[kind], arrived.at[slot], device)

    def move_route(kind, block, device):
        return remote(
            routes.at[block], routes.at[block], rsent.at[kind], routed.at[block], device
        )

    def hand(kind, slot, block, first, device):
        move(kind, slot, device).start()
        pl.when(first)(lambda: move_route(kind, block, device).start())

    weight_loads = [
        pltpu.make_async_copy(gate_hbm.at[0], gate, wsem.at[0]),
        pltpu.make_async_copy(up_hbm.at[0], up, wsem.at[1]),
        pltpu.make_async_copy(down_hbm.at[0], down, wsem.at[2]),
    ]
    for load in weight_loads:
        load.start()

    barrier = pltpu.get_barrier_semaphore()

    def greet(device):
        pl.semaphore_signal(barrier, inc=1, device_id={"ep": device}, device_id_type=MESH)

    greet(ypeer)
    greet(cpeer)
    greet(above)
    pl.when(jnp.logical_not(is_end))(lambda: greet(below))

    for e in range(PLANES):
        routes[me, e : e + 1, :] = jnp.sum(
            jnp.where(ids_ref[...] == e, route_ref[...], 0.0), axis=0, keepdims=True
        )

    def open_step(s, _):
        span = pl.ds(pl.multiple_of(s * piece_rows, piece_rows), piece_rows)
        values = tokens_ref[span, :].astype(jnp.float32)
        center = values - jnp.mean(values, axis=-1, keepdims=True)
        spread = jnp.mean(center * center, axis=-1, keepdims=True)
        slot = me * PIECES + s
        tok[slot] = (center * lax.rsqrt(spread + EPSILON) * gain_ref[...]).astype(jnp.bfloat16)

        @pl.when(s == 0)
        def _():
            pl.semaphore_wait(barrier, jnp.where(is_end, 3, 4))

        hand(1, slot, me, s == 0, above)
        pl.when(jnp.logical_not(is_end))(lambda: hand(2, slot, me, s == 0, below))
        hand(3, slot, me, s == 0, cpeer)
        return 0

    lax.fori_loop(0, PIECES, open_step, 0)
    for load in weight_loads:
        load.wait()

    def relay(h, o, s, entry):
        block = plane_of(h) * 4 + column_of(o) * 2 + c
        slot = block * PIECES + s
        move(3, slot, cpeer).wait_recv()
        pl.when(s == 0)(lambda: move_route(3, block, cpeer).wait_recv())
        pl.when((entry >> 8) & 1 == 1)(lambda: hand(1, slot, block, s == 0, above))
        pl.when((entry >> 9) & 1 == 1)(lambda: hand(2, slot, block, s == 0, below))
        hand(3, slot, block, s == 0, cpeer)

    def cross(h, s):
        block = plane_of(h) * 4 + y * 2 + c
        hand(0, block * PIECES + s, block, s == 0, ypeer)

    def share(pair, s):
        return remote(
            part.at[(pair * 2 + 1 - c) * PIECES + s], cbuf.at[pair * PIECES + s],
            sent.at[4], shared.at[pair * PIECES + s], cpeer,
        )

    def compute(h, o, s, entry):
        h2, o2, s2 = (entry >> 8) & 3, (entry >> 10) & 1, (entry >> 11) & 3
        pairs = [(plane_of(h) * 2 + column_of(o), s), (plane_of(h2) * 2 + column_of(o2), s2)]
        for n, (pair, piece) in enumerate(pairs):
            block = pair * 2 + 1 - c
            move(3, block * PIECES + piece, cpeer).wait_recv()
            pl.when((entry >> (13 + n)) & 1 == 1)(
                lambda block=block: move_route(3, block, cpeer).wait_recv()
            )
        places = [
            ((pair * 2 + core) * PIECES + piece, pair * 2 + core, piece)
            for pair, piece in pairs
            for core in range(2)
        ]
        x = jnp.concatenate([tok[slot] for slot, _, _ in places], axis=0)
        scale = jnp.concatenate(
            [
                lane_column(routes[block, pl.ds(z, 1), :], piece, piece_rows)
                for _, block, piece in places
            ],
            axis=0,
        )
        gate_cut = jnp.minimum(
            jnp.dot(x, gate[...], preferred_element_type=jnp.float32), clamp_limit
        )
        up_cut = jnp.clip(
            jnp.dot(x, up[...], preferred_element_type=jnp.float32), -clamp_limit, clamp_limit
        )
        active = ((up_cut + 1.0) * (gate_cut * jax.nn.sigmoid(gate_cut * sigmoid_slope))).astype(
            jnp.bfloat16
        )
        tile = min(512, width)
        for start in range(0, width, tile):
            value = scale * jnp.dot(
                active, down[:, start : start + tile], preferred_element_type=jnp.float32
            )
            value = value.astype(jnp.bfloat16)
            for n, (slot, _, _) in enumerate(places):
                part[slot, :, start : start + tile] = value[n * piece_rows : (n + 1) * piece_rows]
        for pair, piece in pairs:
            share(pair, piece).start()

    def settle(h, o, s, entry):
        plane = plane_of(h)
        pair = plane * 2 + column_of(o)
        slot = (pair * 2 + c) * PIECES + s
        rank = (plane * 2 + o) * PIECES + s
        lane = pair * PIECES + s
        row = plane * PIECES + s
        share(pair, s).wait_recv()
        acc[...] = part[slot].astype(jnp.float32) + cbuf[lane].astype(jnp.float32)

        def upon(side):
            return side * (2 * PLANES * PIECES) + rank

        def climb(side, device):
            return remote(
                part.at[slot], zbuf.at[upon(side)], sent.at[5], climbed.at[upon(side)], device
            )

        def over():
            return remote(part.at[slot], ybuf.at[row], sent.at[5], crossed.at[row], ypeer)

        @pl.when((entry >> 8) & 1 == 1)
        def _():
            over().wait_recv()
            acc[...] += ybuf[row].astype(jnp.float32)

        for bit, side, device in ((9, 1 - flipped, above), (10, flipped, below)):
            @pl.when((entry >> bit) & 1 == 1)
            def _():
                climb(side, device).wait_recv()
                acc[...] += zbuf[upon(side)].astype(jnp.float32)

        goal = (entry >> 11) & 3

        @pl.when(goal == 3)
        def _():
            out_ref[pl.ds(pl.multiple_of(s * piece_rows, piece_rows), piece_rows), :] = (
                acc[...].astype(jnp.bfloat16)
            )

        @pl.when(goal != 3)
        def _():
            part[slot] = acc[...].astype(jnp.bfloat16)

        pl.when(goal == 0)(lambda: over().start())
        pl.when(goal == 1)(lambda: climb(flipped, above).start())
        pl.when(goal == 2)(lambda: climb(1 - flipped, below).start())

    groups = max(len(END_WORDS), len(MID_WORDS)) // (GROUP // 2)

    def group_step(g, _):
        words = []
        for n in range(GROUP // 2):
            word = jnp.where(is_end, END_WORDS[n], MID_WORDS[n])
            for k in range(1, groups):
                at = k * (GROUP // 2) + n
                word = jnp.where(g == k, jnp.where(is_end, END_WORDS[at], MID_WORDS[at]), word)
            words.append(word)

        def entry_step(j, _):
            word = words[0]
            for n in range(1, GROUP // 2):
                word = jnp.where(j // 2 == n, words[n], word)
            entry = jnp.where(j % 2 == 0, word & 32767, word >> 15)
            kind = entry & 7
            h, o, s = (entry >> 3) & 3, (entry >> 5) & 1, (entry >> 6) & 3
            pl.when(kind == RELAY)(lambda: relay(h, o, s, entry))
            pl.when(kind == CROSS)(lambda: cross(h, s))
            pl.when(kind == COMPUTE)(lambda: compute(h, o, s, entry))
            pl.when(kind == SETTLE)(lambda: settle(h, o, s, entry))
            return 0

        lax.fori_loop(0, GROUP, entry_step, 0)
        return 0

    lax.fori_loop(0, groups, group_step, 0)

    def drain(counts, tiles):
        for kind, count in enumerate(counts):
            if count:
                whole = tok.at[pl.ds(0, count)]
                pltpu.make_async_copy(whole, whole, sent.at[kind]).wait()
        for kind, count in enumerate(tiles):
            if count:
                whole = routes.at[pl.ds(0, count)]
                pltpu.make_async_copy(whole, whole, rsent.at[kind]).wait()

    pl.when(is_end)(lambda: drain(END_SENT, END_TILES))
    pl.when(jnp.logical_not(is_end))(lambda: drain(MID_SENT, MID_TILES))


def dense_body(tokens, norm_gain, expert_ids, route_weight, gate_weight, up_weight, down_weight):
    devices = lax.axis_size("ep")
    rows, width = tokens.shape
    hidden = gate_weight.shape[2]
    piece_rows = rows // PIECES
    vmem, dma = pltpu.VMEM, pltpu.SemaphoreType.DMA
    block = jnp.bfloat16
    lanes = devices // 2 * PIECES
    return pl.pallas_call(
        dense_kernel,
        out_shape=jax.ShapeDtypeStruct((rows, width), block),
        in_specs=[pl.BlockSpec(memory_space=vmem)] * 4 + [pl.BlockSpec(memory_space=pl.ANY)] * 3,
        out_specs=pl.BlockSpec(memory_space=vmem),
        scratch_shapes=[
            vmem((devices * PIECES, piece_rows, width), block),
            vmem((devices * PIECES, piece_rows, width), block),
            vmem((lanes, piece_rows, width), block),
            vmem((PLANES * PIECES, piece_rows, width), block),
            vmem((4 * PLANES * PIECES, piece_rows, width), block),
            vmem((piece_rows, width), jnp.float32),
            vmem((devices, 8, rows), jnp.float32),
            vmem((width, hidden), block),
            vmem((width, hidden), block),
            vmem((hidden, width), block),
            dma((3,)),
            dma((devices * PIECES,)),
            dma((devices,)),
            dma((lanes,)),
            dma((PLANES * PIECES,)),
            dma((4 * PLANES * PIECES,)),
            dma((6,)),
            dma((4,)),
        ],
        compiler_params=pltpu.CompilerParams(
            collective_id=0, has_side_effects=True, vmem_limit_bytes=60 * 1024 * 1024
        ),
        name="dense_experts",
    )(
        tokens, norm_gain.reshape(1, width), expert_ids.T, route_weight.T,
        gate_weight, up_weight, down_weight,
    )


def body(tokens, norm_gain, expert_ids, route_weight, gate_weight, up_weight, down_weight):
    tok_rows, top_count = expert_ids.shape
    experts = lax.axis_size("ep") // SPLIT
    capacity = min(tok_rows, 2 * tok_rows * top_count // experts)
    dense = capacity == tok_rows and experts == PLANES and tok_rows % (16 * PIECES) == 0
    chosen = dense_body if dense else slot_body
    return chosen(
        tokens, norm_gain, expert_ids, route_weight, gate_weight, up_weight, down_weight
    )


def solution(mesh):
    placed = (
        P(("grp", "ep"), None),
        P(),
        P(("grp", "ep"), None),
        P(("grp", "ep"), None),
        P("ep", None, None),
        P("ep", None, None),
        P("ep", None, None),
    )
    return jax.shard_map(
        body, mesh=mesh, in_specs=placed, out_specs=P(("grp", "ep"), None), check_vma=False
    )
```

time: 104 us -> 77.4 us (0.74)
  Pallas kernels: 102 us -> 75.3 us
    pallas_call x1, Pallas kernels: 102 us -> 75.3 us  [dense_body(): pl.pallas_call(dense_kernel, out_shape=jax.ShapeDtypeStruct((rows, width)...]
where the time goes in v1:
time: 77.4 us; the launch traced here: 77.2 us
  Pallas kernels  75.3 us (97%)
  local copies, waits for them, and re-layouts  1.88 us (2%)
    pallas_call x1, Pallas kernels, dense_body(): pl.pallas_call(dense_kernel, out_shape=jax.ShapeDtypeStruct((rows, width)...  75.3 us
    unnamed x1, local copies, waits for them, and re-layouts  1.88 us

profile of v1, /device:TPU:0, one launch (start us, length us, event | category | flops | bytes accessed | tf_op | source)
XLA Modules:
  0.0 77.2 jit_solution(4073533361755891644)
XLA Ops:
  0.0 75.3 %dense_experts.1 = bf16[128,2048]{1,0:T(8,128)(2,1)} custom-call(bf16[128,2048]{1,0:T(8,128)(2,1)} %tokens_ref.1, f32[1,2048]{1,0:T(1,128)} %bitcast.3, s32[2,128]{1,0:T(2,128)} %bitcast.4, f32[2,128]{1,0:T(2,128)} %bitcast.5, bf16[1,2048,512]{2,1,0:T(8,128)(2,1)} %gate_hbm.1, bf16[1,2048,512]{2,1,0:T(8,128)(2,1)} %up_hbm.1, bf16[1,512,2048]{2,1,0:T(8,128)(2,1)} %down_hbm.1), custom_call_target="tpu_custom_call" | custom-call | tf_op jit(solution)/shard_map/dense_experts/pallas_call | solution.py:369
  75.3 1.9 %copy.9 = bf16[128,2048]{1,0:T(8,128)(2,1)} copy(bf16[128,2048]{1,0:T(8,128)(2,1)} %dense_experts.1) | data formatting | bytes 1048576

commit v2 on v1

--- a/solution.py
+++ b/solution.py
@@ -122,12 +122,12 @@
 
 
 def dense_kernel(
-    tokens_ref, gain_ref, ids_ref, route_ref, gate_hbm, up_hbm, down_hbm,
+    tokens_hbm, gain_hbm, ids_hbm, route_hbm, gate_hbm, up_hbm, down_hbm,
     out_ref,
-    tok, part, cbuf, ybuf, zbuf, acc, routes, gate, up, down,
-    wsem, arrived, routed, shared, crossed, climbed, sent, rsent,
+    tok, part, cbuf, ybuf, zbuf, acc, routes, tokens, gain, ids, route, gate, up, down,
+    lsem, wsem, arrived, routed, shared, crossed, climbed, sent, rsent,
 ):
-    rows, width = tokens_ref.shape
+    rows, width = tokens_hbm.shape
     piece_rows = rows // PIECES
     me = lax.axis_index("ep")
     z, y, c = me // 4, (me // 2) % 2, me % 2
@@ -162,14 +162,6 @@
         move(kind, slot, device).start()
         pl.when(first)(lambda: move_route(kind, block, device).start())
 
-    weight_loads = [
-        pltpu.make_async_copy(gate_hbm.at[0], gate, wsem.at[0]),
-        pltpu.make_async_copy(up_hbm.at[0], up, wsem.at[1]),
-        pltpu.make_async_copy(down_hbm.at[0], down, wsem.at[2]),
-    ]
-    for load in weight_loads:
-        load.start()
-
     barrier = pltpu.get_barrier_semaphore()
 
     def greet(device):
@@ -180,18 +172,40 @@
     greet(above)
     pl.when(jnp.logical_not(is_end))(lambda: greet(below))
 
+    def load_piece(s):
+        span = pl.ds(pl.multiple_of(s * piece_rows, piece_rows), piece_rows)
+        return pltpu.make_async_copy(tokens_hbm.at[span], tokens.at[span], wsem.at[s])
+
+    small_loads = [
+        pltpu.make_async_copy(ids_hbm, ids, lsem.at[0]),
+        pltpu.make_async_copy(route_hbm, route, lsem.at[1]),
+        pltpu.make_async_copy(gain_hbm, gain, lsem.at[2]),
+    ]
+    weight_loads = [
+        pltpu.make_async_copy(gate_hbm.at[0], gate, lsem.at[3]),
+        pltpu.make_async_copy(up_hbm.at[0], up, lsem.at[4]),
+        pltpu.make_async_copy(down_hbm.at[0], down, lsem.at[5]),
+    ]
+    for s in range(PIECES):
+        load_piece(s).start()
+    for load in small_loads + weight_loads:
+        load.start()
+
+    for load in small_loads:
+        load.wait()
     for e in range(PLANES):
         routes[me, e : e + 1, :] = jnp.sum(
-            jnp.where(ids_ref[...] == e, route_ref[...], 0.0), axis=0, keepdims=True
+            jnp.where(ids[...] == e, route[...], 0.0), axis=0, keepdims=True
         )
 
     def open_step(s, _):
         span = pl.ds(pl.multiple_of(s * piece_rows, piece_rows), piece_rows)
-        values = tokens_ref[span, :].astype(jnp.float32)
+        load_piece(s).wait()
+        values = tokens[span, :].astype(jnp.float32)
         center = values - jnp.mean(values, axis=-1, keepdims=True)
         spread = jnp.mean(center * center, axis=-1, keepdims=True)
         slot = me * PIECES + s
-        tok[slot] = (center * lax.rsqrt(spread + EPSILON) * gain_ref[...]).astype(jnp.bfloat16)
+        tok[slot] = (center * lax.rsqrt(spread + EPSILON) * gain[...]).astype(jnp.bfloat16)
 
         @pl.when(s == 0)
         def _():
@@ -361,6 +375,7 @@
 def dense_body(tokens, norm_gain, expert_ids, route_weight, gate_weight, up_weight, down_weight):
     devices = lax.axis_size("ep")
     rows, width = tokens.shape
+    top = expert_ids.shape[1]
     hidden = gate_weight.shape[2]
     piece_rows = rows // PIECES
     vmem, dma = pltpu.VMEM, pltpu.SemaphoreType.DMA
@@ -369,7 +384,7 @@
     return pl.pallas_call(
         dense_kernel,
         out_shape=jax.ShapeDtypeStruct((rows, width), block),
-        in_specs=[pl.BlockSpec(memory_space=vmem)] * 4 + [pl.BlockSpec(memory_space=pl.ANY)] * 3,
+        in_specs=[pl.BlockSpec(memory_space=pltpu.HBM)] * 7,
         out_specs=pl.BlockSpec(memory_space=vmem),
         scratch_shapes=[
             vmem((devices * PIECES, piece_rows, width), block),
@@ -379,10 +394,15 @@
             vmem((4 * PLANES * PIECES, piece_rows, width), block),
             vmem((piece_rows, width), jnp.float32),
             vmem((devices, 8, rows), jnp.float32),
+            vmem((rows, width), block),
+            vmem((1, width), jnp.float32),
+            vmem((top, rows), jnp.int32),
+            vmem((top, rows), jnp.float32),
             vmem((width, hidden), block),
             vmem((width, hidden), block),
             vmem((hidden, width), block),
-            dma((3,)),
+            dma((6,)),
+            dma((PIECES,)),
             dma((devices * PIECES,)),
             dma((devices,)),
             dma((lanes,)),
@@ -392,12 +412,17 @@
             dma((4,)),
         ],
         compiler_params=pltpu.CompilerParams(
-            collective_id=0, has_side_effects=True, vmem_limit_bytes=60 * 1024 * 1024
+            collective_id=0, has_side_effects=True, vmem_limit_bytes=40 * 1024 * 1024
         ),
         name="dense_experts",
     )(
-        tokens, norm_gain.reshape(1, width), expert_ids.T, route_weight.T,
-        gate_weight, up_weight, down_weight,
+        *[
+            pltpu.with_memory_space_constraint(array, pltpu.HBM)
+            for array in (
+                tokens, norm_gain.reshape(1, width), expert_ids.T, route_weight.T,
+                gate_weight, up_weight, down_weight,
+            )
+        ]
     )
 
 

time: 77.4 us -> 74.8 us (0.966)
  Pallas kernels: 75.3 us -> 73.8 us
  local copies, waits for them, and re-layouts: 1.88 us -> 0.8 us
    pallas_call x1, Pallas kernels: 75.3 us -> 73.8 us  [dense_body(): pl.pallas_call(dense_kernel, out_shape=jax.ShapeDtypeStruct((rows, width)...]
    unnamed x1, local copies, waits for them, and re-layouts: 1.88 us -> 0.8 us
where the time goes in v2:
time: 74.8 us; the launch traced here: 74.6 us
  Pallas kernels  73.8 us (99%)
  local copies, waits for them, and re-layouts  0.8 us (1%)
    pallas_call x1, Pallas kernels, dense_body(): pl.pallas_call(dense_kernel, out_shape=jax.ShapeDtypeStruct((rows, width)...  73.8 us

profile of v2, /device:TPU:0, one launch (start us, length us, event | category | flops | bytes accessed | tf_op | source)
XLA Modules:
  0.0 74.6 jit_solution(1016188180379453419)
XLA Ops:
  0.0 73.8 %dense_experts.1 = bf16[128,2048]{1,0:T(8,128)(2,1)S(1)} custom-call(bf16[128,2048]{1,0:T(8,128)(2,1)} %tokens_hbm.1, f32[1,2048]{1,0:T(1,128)} %bitcast.3, s32[2,128]{1,0:T(2,128)} %bitcast.4, f32[2,128]{1,0:T(2,128)} %bitcast.5, bf16[1,2048,512]{2,1,0:T(8,128)(2,1)} %gate_hbm.1, bf16[1,2048,512]{2,1,0:T(8,128)(2,1)} %up_hbm.1, bf16[1,512,2048]{2,1,0:T(8,128)(2,1)} %down_hbm.1), custom_call_target="tpu_custom_call" | custom-call | tf_op jit(solution)/shard_map/dense_experts/pallas_call | solution.py:384
  73.8 0.8 %copy.9 = bf16[128,2048]{1,0:T(8,128)(2,1)} copy(bf16[128,2048]{1,0:T(8,128)(2,1)S(1)} %dense_experts.1) | data formatting | bytes 1048576

commit v3 on v2

--- a/solution.py
+++ b/solution.py
@@ -90,24 +90,24 @@
 RELAY, CROSS, COMPUTE, SETTLE = 0, 1, 2, 3
 GROUP = 8
 END_WORDS = (
-    32897, 262209, 335609865, 2373642, 13631520, 11534409,
-    6341706, 1312779, 557072, 69566664, 6612242, 7340112,
-    3408008, 67731480, 170459161, 68517936, 7110872, 2657386,
-    69828745, 300744936, 1837163, 5347714, 8126648, 74311474,
-    6815864, 201130096, 68780272, 121438267, 75333784, 259063995,
-    4032627, 166264920, 5767411, 1149211, 98109851, 5505168,
-    5870058, 82413915, 7706002, 80314539, 82150115, 80052835,
-    230791939, 228694979,
+    2130049, 294920, 470099970, 1048648, 2392480, 572850528,
+    67469505, 524328, 6553617, 847841355, 2621641, 4456672,
+    786536, 821267, 1578066, 7079979, 104136921, 4489297,
+    7604307, 70624218, 213975096, 6029475, 865665272, 3934427,
+    3670224, 7870458, 1935411, 4984442, 6129915, 70885090,
+    2883707, 7967698, 76382384, 80576547, 4721586, 150274216,
+    78479539, 180947411, 5603563, 24218003, 20023755, 226593163,
+    232889219, 138051,
 )
 MID_WORDS = (
-    6586377, 8388648, 279248897, 557584, 19411242, 14680201,
-    6340810, 17563680, 7602592, 11534361, 1573592, 23606306,
-    10485969, 300744921, 2654264, 22806912, 20709800, 245965522,
-    101297978, 24641609, 5344442, 69042424, 3670680, 7700704,
-    103388610, 3408472, 326697648, 21495931, 6131811, 263785691,
-    102335011, 108893786, 239927539, 104436419, 111216171, 5868571,
-    158438018, 53841307, 112041739, 115970819, 5608323, 113876811,
-    266703427, 139147,
+    1310921, 33024, 17310026, 412418065, 4489808, 543490496,
+    1048769, 13632024, 819432, 23855456, 437321776, 6849232,
+    7110976, 1844186, 12582993, 13894328, 292094584, 396172626,
+    2395155, 106758896, 8126627, 21760059, 7340144, 182517995,
+    19663955, 22544488, 4040434, 137462416, 107839675, 17932146,
+    187501619, 7965947, 157392026, 51743859, 101551426, 155254963,
+    114135779, 260408939, 159485275, 163679699, 262504619, 153193875,
+    264609739, 131076,
 )
 END_SENT = (12, 6, 0, 32, 32, 28)
 END_TILES = (4, 1, 0, 8)
@@ -213,6 +213,7 @@
 
         hand(1, slot, me, s == 0, above)
         pl.when(jnp.logical_not(is_end))(lambda: hand(2, slot, me, s == 0, below))
+        pl.when(s == 0)(lambda: hand(0, slot, me, True, ypeer))
         hand(3, slot, me, s == 0, cpeer)
         return 0
 
@@ -393,7 +394,7 @@
             vmem((PLANES * PIECES, piece_rows, width), block),
             vmem((4 * PLANES * PIECES, piece_rows, width), block),
             vmem((piece_rows, width), jnp.float32),
-            vmem((devices, 8, rows), jnp.float32),
+            vmem((devices, PLANES, rows), jnp.float32),
             vmem((rows, width), block),
             vmem((1, width), jnp.float32),
             vmem((top, rows), jnp.int32),

time: 74.8 us -> 73.1 us (0.977)
  Pallas kernels: 73.8 us -> 72.1 us
    pallas_call x1, Pallas kernels: 73.8 us -> 72.1 us  [dense_body(): pl.pallas_call(dense_kernel, out_shape=jax.ShapeDtypeStruct((rows, width)...]
where the time goes in v3:
time: 73.1 us; the launch traced here: 72.9 us
  Pallas kernels  72.1 us (99%)
  local copies, waits for them, and re-layouts  0.8 us (1%)
    pallas_call x1, Pallas kernels, dense_body(): pl.pallas_call(dense_kernel, out_shape=jax.ShapeDtypeStruct((rows, width)...  72.1 us

profile of v3, /device:TPU:0, one launch (start us, length us, event | category | flops | bytes accessed | tf_op | source)
XLA Modules:
  0.0 72.9 jit_solution(11845760565405223671)
XLA Ops:
  0.0 72.1 %dense_experts.1 = bf16[128,2048]{1,0:T(8,128)(2,1)S(1)} custom-call(bf16[128,2048]{1,0:T(8,128)(2,1)} %tokens_hbm.1, f32[1,2048]{1,0:T(1,128)} %bitcast.3, s32[2,128]{1,0:T(2,128)} %bitcast.4, f32[2,128]{1,0:T(2,128)} %bitcast.5, bf16[1,2048,512]{2,1,0:T(8,128)(2,1)} %gate_hbm.1, bf16[1,2048,512]{2,1,0:T(8,128)(2,1)} %up_hbm.1, bf16[1,512,2048]{2,1,0:T(8,128)(2,1)} %down_hbm.1), custom_call_target="tpu_custom_call" | custom-call | tf_op jit(solution)/shard_map/dense_experts/pallas_call | solution.py:385
  72.1 0.8 %copy.9 = bf16[128,2048]{1,0:T(8,128)(2,1)} copy(bf16[128,2048]{1,0:T(8,128)(2,1)S(1)} %dense_experts.1) | data formatting | bytes 1048576

commit v4 on v3

--- a/solution.py
+++ b/solution.py
@@ -90,28 +90,28 @@
 RELAY, CROSS, COMPUTE, SETTLE = 0, 1, 2, 3
 GROUP = 8
 END_WORDS = (
-    2130049, 294920, 470099970, 1048648, 2392480, 572850528,
-    67469505, 524328, 6553617, 847841355, 2621641, 4456672,
-    786536, 821267, 1578066, 7079979, 104136921, 4489297,
-    7604307, 70624218, 213975096, 6029475, 865665272, 3934427,
-    3670224, 7870458, 1935411, 4984442, 6129915, 70885090,
-    2883707, 7967698, 76382384, 80576547, 4721586, 150274216,
-    78479539, 180947411, 5603563, 24218003, 20023755, 226593163,
-    232889219, 138051,
+    6324353, 1048584, 13631497, 4489352, 805634528, 148963393,
+    67469352, 557072, 71689506, 2654288, 555810984, 819224,
+    1574955, 67734242, 2916440, 592773320, 69828809, 3670072,
+    7438544, 600901803, 6029432, 68797298, 8126523, 1153402,
+    7866483, 608016378, 100204760, 3145979, 7604507, 5767355,
+    346921690, 7962776, 82679530, 4721818, 5865544, 80576747,
+    139001960, 111479251, 3508627, 82156291, 22127203, 232884555,
+    230792003, 131076,
 )
 MID_WORDS = (
-    1310921, 33024, 17310026, 412418065, 4489808, 543490496,
-    1048769, 13632024, 819432, 23855456, 437321776, 6849232,
-    7110976, 1844186, 12582993, 13894328, 292094584, 396172626,
-    2395155, 106758896, 8126627, 21760059, 7340144, 182517995,
-    19663955, 22544488, 4040434, 137462416, 107839675, 17932146,
-    187501619, 7965947, 157392026, 51743859, 101551426, 155254963,
-    114135779, 260408939, 159485275, 163679699, 262504619, 153193875,
-    264609739, 131076,
+    8388809, 17301505, 805634065, 4489808, 2130240, 88418322,
+    1048616, 819736, 1573280, 23593560, 2654688, 13893841,
+    504181794, 7602272, 14680120, 22806912, 488177737, 2916464,
+    1147640, 24641763, 23866426, 587009043, 207422128, 103383160,
+    1933976, 96010896, 188811451, 8227891, 20191610, 256725091,
+    306023539, 51748314, 109936883, 156340842, 81071451, 159482035,
+    260410843, 39170883, 7703707, 115966571, 113873859, 266703491,
+    262512523, 131076,
 )
-END_SENT = (12, 6, 0, 32, 32, 28)
+END_SENT = (11, 6, 0, 32, 32, 28)
 END_TILES = (4, 1, 0, 8)
-MID_SENT = (11, 11, 16, 32, 32, 28)
+MID_SENT = (11, 11, 17, 32, 32, 28)
 MID_TILES = (4, 2, 3, 8)
 
 
@@ -289,30 +289,44 @@
         rank = (plane * 2 + o) * PIECES + s
         lane = pair * PIECES + s
         row = plane * PIECES + s
+        whole, first, second = (
+            pl.ds(0, piece_rows), pl.ds(0, piece_rows // 2), pl.ds(piece_rows // 2, piece_rows // 2)
+        )
         share(pair, s).wait_recv()
         acc[...] = part[slot].astype(jnp.float32) + cbuf[lane].astype(jnp.float32)
 
         def upon(side):
             return side * (2 * PLANES * PIECES) + rank
 
-        def climb(side, device):
+        def climb(side, device, span):
             return remote(
-                part.at[slot], zbuf.at[upon(side)], sent.at[5], climbed.at[upon(side)], device
-            )
-
-        def over():
-            return remote(part.at[slot], ybuf.at[row], sent.at[5], crossed.at[row], ypeer)
-
-        @pl.when((entry >> 8) & 1 == 1)
-        def _():
-            over().wait_recv()
-            acc[...] += ybuf[row].astype(jnp.float32)
-
+                part.at[slot, span], zbuf.at[upon(side), span],
+                sent.at[5], climbed.at[upon(side)], device,
+            )
+
+        def over(span):
+            return remote(
+                part.at[slot, span], ybuf.at[row, span], sent.at[5], crossed.at[row], ypeer
+            )
+
+        def take(comes, halved, half, copy, buffer, at):
+            for span, wanted in (
+                (whole, jnp.logical_and(comes, jnp.logical_not(halved))),
+                (half, jnp.logical_and(comes, halved)),
+            ):
+                @pl.when(wanted)
+                def _(span=span):
+                    copy(span).wait_recv()
+                    acc[span, :] += buffer[at, span, :].astype(jnp.float32)
+
+        halved = (entry >> 13) & 1 == 1
+        take((entry >> 8) & 1 == 1, halved, first, over, ybuf, row)
         for bit, side, device in ((9, 1 - flipped, above), (10, flipped, below)):
-            @pl.when((entry >> bit) & 1 == 1)
-            def _():
-                climb(side, device).wait_recv()
-                acc[...] += zbuf[upon(side)].astype(jnp.float32)
+            take(
+                (entry >> bit) & 1 == 1, jnp.logical_and(halved, o == 1), second,
+                lambda span, side=side, device=device: climb(side, device, span),
+                zbuf, upon(side),
+            )
 
         goal = (entry >> 11) & 3
 
@@ -326,9 +340,14 @@
         def _():
             part[slot] = acc[...].astype(jnp.bfloat16)
 
-        pl.when(goal == 0)(lambda: over().start())
-        pl.when(goal == 1)(lambda: climb(flipped, above).start())
-        pl.when(goal == 2)(lambda: climb(1 - flipped, below).start())
+        split = (entry >> 14) & 1 == 1
+        pl.when(goal == 0)(lambda: over(whole).start())
+        pl.when(split)(lambda: over(first).start())
+        for way, side, device in ((1, flipped, above), (2, 1 - flipped, below)):
+            for span, wanted in ((whole, jnp.logical_not(split)), (second, split)):
+                pl.when(jnp.logical_and(goal == way, wanted))(
+                    lambda side=side, device=device, span=span: climb(side, device, span).start()
+                )
 
     groups = max(len(END_WORDS), len(MID_WORDS)) // (GROUP // 2)
 
@@ -431,7 +450,7 @@
     tok_rows, top_count = expert_ids.shape
     experts = lax.axis_size("ep") // SPLIT
     capacity = min(tok_rows, 2 * tok_rows * top_count // experts)
-    dense = capacity == tok_rows and experts == PLANES and tok_rows % (16 * PIECES) == 0
+    dense = capacity == tok_rows and experts == PLANES and tok_rows % (32 * PIECES) == 0
     chosen = dense_body if dense else slot_body
     return chosen(
         tokens, norm_gain, expert_ids, route_weight, gate_weight, up_weight, down_weight

time: 73.1 us -> 72.4 us (level)
  no operation moved by 1% of the time
where the time goes in v4:
time: 72.4 us; the launch traced here: 72.2 us
  Pallas kernels  71.4 us (99%)
  local copies, waits for them, and re-layouts  0.8 us (1%)
    pallas_call x1, Pallas kernels, dense_body(): pl.pallas_call(dense_kernel, out_shape=jax.ShapeDtypeStruct((rows, width)...  71.4 us

profile of v4, /device:TPU:0, one launch (start us, length us, event | category | flops | bytes accessed | tf_op | source)
XLA Modules:
  0.0 72.2 jit_solution(1827539863121011948)
XLA Ops:
  0.0 71.4 %dense_experts.1 = bf16[128,2048]{1,0:T(8,128)(2,1)S(1)} custom-call(bf16[128,2048]{1,0:T(8,128)(2,1)} %tokens_hbm.1, f32[1,2048]{1,0:T(1,128)} %bitcast.3, s32[2,128]{1,0:T(2,128)} %bitcast.4, f32[2,128]{1,0:T(2,128)} %bitcast.5, bf16[1,2048,512]{2,1,0:T(8,128)(2,1)} %gate_hbm.1, bf16[1,2048,512]{2,1,0:T(8,128)(2,1)} %up_hbm.1, bf16[1,512,2048]{2,1,0:T(8,128)(2,1)} %down_hbm.1), custom_call_target="tpu_custom_call" | custom-call | tf_op jit(solution)/shard_map/dense_experts/pallas_call | solution.py:404
  71.4 0.8 %copy.9 = bf16[128,2048]{1,0:T(8,128)(2,1)} copy(bf16[128,2048]{1,0:T(8,128)(2,1)S(1)} %dense_experts.1) | data formatting | bytes 1048576

commit v5 on v4

--- a/solution.py
+++ b/solution.py
@@ -90,28 +90,28 @@
 RELAY, CROSS, COMPUTE, SETTLE = 0, 1, 2, 3
 GROUP = 8
 END_WORDS = (
-    6324353, 1048584, 13631497, 4489352, 805634528, 148963393,
-    67469352, 557072, 71689506, 2654288, 555810984, 819224,
-    1574955, 67734242, 2916440, 592773320, 69828809, 3670072,
-    7438544, 600901803, 6029432, 68797298, 8126523, 1153402,
-    7866483, 608016378, 100204760, 3145979, 7604507, 5767355,
-    346921690, 7962776, 82679530, 4721818, 5865544, 80576747,
-    139001960, 111479251, 3508627, 82156291, 22127203, 232884555,
-    230792003, 131076,
+    262337, 4227081, 2392136, 15728672, 1335306, 4458507,
+    345309321, 524488, 68517905, 69566568, 4732946, 573898897,
+    788499, 1572889, 5509858, 2885739, 832110681, 6817939,
+    1835217, 1147056, 68785498, 8126624, 3932225, 6047666,
+    7866459, 72978426, 257753147, 8224880, 7080059, 611942587,
+    4980832, 76389330, 5608306, 7604699, 80576592, 108331123,
+    350851410, 211886819, 78217451, 172034443, 22119011, 226593227,
+    232889155, 138115,
 )
 MID_WORDS = (
-    8388809, 17301505, 805634065, 4489808, 2130240, 88418322,
-    1048616, 819736, 1573280, 23593560, 2654688, 13893841,
-    504181794, 7602272, 14680120, 22806912, 488177737, 2916464,
-    1147640, 24641763, 23866426, 587009043, 207422128, 103383160,
-    1933976, 96010896, 188811451, 8227891, 20191610, 256725091,
-    306023539, 51748314, 109936883, 156340842, 81071451, 159482035,
-    260410843, 39170883, 7703707, 115966571, 113873859, 266703491,
-    262512523, 131076,
+    8388681, 1310721, 4497866, 847315472, 557376, 1048960,
+    21495937, 819736, 15728705, 411631664, 856752728, 4751776,
+    11796648, 14680265, 296551120, 2916408, 239665912, 5767864,
+    530385939, 20447441, 8227138, 21758680, 3146472, 105480251,
+    1147000, 190644816, 163384371, 120672483, 231803995, 51743923,
+    6127731, 182518000, 139562107, 255922755, 260410651, 309960018,
+    154242523, 221577899, 159485339, 115967083, 7713731, 155290963,
+    262512523, 139211,
 )
-END_SENT = (11, 6, 0, 32, 32, 28)
+END_SENT = (12, 5, 0, 32, 32, 28)
 END_TILES = (4, 1, 0, 8)
-MID_SENT = (11, 11, 17, 32, 32, 28)
+MID_SENT = (12, 11, 16, 32, 32, 28)
 MID_TILES = (4, 2, 3, 8)
 
 

time: 72.4 us -> 71.9 us (level)
  no operation moved by 1% of the time
where the time goes in v5:
time: 71.9 us; the launch traced here: 71.8 us
  Pallas kernels  71 us (99%)
  local copies, waits for them, and re-layouts  0.8 us (1%)
    pallas_call x1, Pallas kernels, dense_body(): pl.pallas_call(dense_kernel, out_shape=jax.ShapeDtypeStruct((rows, width)...  71 us

profile of v5, /device:TPU:0, one launch (start us, length us, event | category | flops | bytes accessed | tf_op | source)
XLA Modules:
  0.0 71.8 jit_solution(199164325713347202)
XLA Ops:
  0.0 71.0 %dense_experts.1 = bf16[128,2048]{1,0:T(8,128)(2,1)S(1)} custom-call(bf16[128,2048]{1,0:T(8,128)(2,1)} %tokens_hbm.1, f32[1,2048]{1,0:T(1,128)} %bitcast.3, s32[2,128]{1,0:T(2,128)} %bitcast.4, f32[2,128]{1,0:T(2,128)} %bitcast.5, bf16[1,2048,512]{2,1,0:T(8,128)(2,1)} %gate_hbm.1, bf16[1,2048,512]{2,1,0:T(8,128)(2,1)} %up_hbm.1, bf16[1,512,2048]{2,1,0:T(8,128)(2,1)} %down_hbm.1), custom_call_target="tpu_custom_call" | custom-call | tf_op jit(solution)/shard_map/dense_experts/pallas_call | solution.py:404
  71.0 0.8 %copy.9 = bf16[128,2048]{1,0:T(8,128)(2,1)} copy(bf16[128,2048]{1,0:T(8,128)(2,1)S(1)} %dense_experts.1) | data formatting | bytes 1048576

commit v6 on v5

--- a/solution.py
+++ b/solution.py
@@ -90,28 +90,28 @@
 RELAY, CROSS, COMPUTE, SETTLE = 0, 1, 2, 3
 GROUP = 8
 END_WORDS = (
-    262337, 4227081, 2392136, 15728672, 1335306, 4458507,
-    345309321, 524488, 68517905, 69566568, 4732946, 573898897,
-    788499, 1572889, 5509858, 2885739, 832110681, 6817939,
-    1835217, 1147056, 68785498, 8126624, 3932225, 6047666,
-    7866459, 72978426, 257753147, 8224880, 7080059, 611942587,
-    4980832, 76389330, 5608306, 7604699, 80576592, 108331123,
-    350851410, 211886819, 78217451, 172034443, 22119011, 226593227,
-    232889155, 138115,
+    262337, 4227081, 2384130, 1048649, 15728680, 203753483,
+    848363585, 557072, 69566568, 2623531, 557121617, 819224,
+    4456496, 237570155, 4982803, 3670169, 1847602, 2916440,
+    6555731, 68780233, 6041146, 5514074, 70877243, 3932408,
+    1151930, 7866459, 6131706, 5245211, 184090840, 7604347,
+    5767419, 7969698, 5605787, 249102544, 82673808, 5867730,
+    7438432, 155257067, 82412195, 80320866, 226592971, 20023691,
+    228694915, 138179,
 )
 MID_WORDS = (
-    8388681, 1310721, 4497866, 847315472, 557376, 1048960,
-    21495937, 819736, 15728705, 411631664, 856752728, 4751776,
-    11796648, 14680265, 296551120, 2916408, 239665912, 5767864,
-    530385939, 20447441, 8227138, 21758680, 3146472, 105480251,
-    1147000, 190644816, 163384371, 120672483, 231803995, 51743923,
-    6127731, 182518000, 139562107, 255922755, 260410651, 309960018,
-    154242523, 221577899, 159485339, 115967083, 7713731, 155290963,
-    262512523, 139211,
+    6586505, 8401162, 2392065, 1311248, 12583504, 847315264,
+    4227560, 17563680, 15728657, 839450728, 819864, 13635810,
+    2654808, 1573312, 2130856, 336396515, 379125816, 24903792,
+    24659802, 6029347, 174392427, 1933664, 101286616, 22550466,
+    102342514, 23597922, 37322939, 3932816, 103651058, 139565690,
+    8228123, 153193595, 91031083, 159485339, 183828723, 116232803,
+    260407475, 155290963, 41255083, 115970634, 113873859, 266706763,
+    139147, 131076,
 )
 END_SENT = (12, 5, 0, 32, 32, 28)
 END_TILES = (4, 1, 0, 8)
-MID_SENT = (12, 11, 16, 32, 32, 28)
+MID_SENT = (10, 13, 16, 32, 32, 28)
 MID_TILES = (4, 2, 3, 8)
 
 

time: 71.9 us -> 71.6 us (level)
  Pallas kernels: 71 us -> 70.2 us
    pallas_call x1, Pallas kernels: 71 us -> 70.2 us  [dense_body(): pl.pallas_call(dense_kernel, out_shape=jax.ShapeDtypeStruct((rows, width)...]
where the time goes in v6:
time: 71.6 us; the launch traced here: 71 us
  Pallas kernels  70.2 us (98%)
  local copies, waits for them, and re-layouts  0.8 us (1%)
    pallas_call x1, Pallas kernels, dense_body(): pl.pallas_call(dense_kernel, out_shape=jax.ShapeDtypeStruct((rows, width)...  70.2 us

profile of v6, /device:TPU:0, one launch (start us, length us, event | category | flops | bytes accessed | tf_op | source)
XLA Modules:
  0.0 71.0 jit_solution(16142091275240358102)
XLA Ops:
  0.0 70.2 %dense_experts.1 = bf16[128,2048]{1,0:T(8,128)(2,1)S(1)} custom-call(bf16[128,2048]{1,0:T(8,128)(2,1)} %tokens_hbm.1, f32[1,2048]{1,0:T(1,128)} %bitcast.3, s32[2,128]{1,0:T(2,128)} %bitcast.4, f32[2,128]{1,0:T(2,128)} %bitcast.5, bf16[1,2048,512]{2,1,0:T(8,128)(2,1)} %gate_hbm.1, bf16[1,2048,512]{2,1,0:T(8,128)(2,1)} %up_hbm.1, bf16[1,512,2048]{2,1,0:T(8,128)(2,1)} %down_hbm.1), custom_call_target="tpu_custom_call" | custom-call | tf_op jit(solution)/shard_map/dense_experts/pallas_call | solution.py:404
  70.2 0.8 %copy.9 = bf16[128,2048]{1,0:T(8,128)(2,1)} copy(bf16[128,2048]{1,0:T(8,128)(2,1)S(1)} %dense_experts.1) | data formatting | bytes 1048576
